TPU v7x, 32 devices: a whole 2x2x4 slice. The times are simulated.
32 devices in a mesh: grp: 2 (over y), ep: 8 (over z, x), tp: 2 (over core).
Axes of the slice: x: 2, y: 2, z: 4, core: 2. Of those that a mesh axis runs over, the one named last changes fastest.
Arguments:
- fresh_inputs: bfloat16 [256, 2048], P(('grp', 'ep')), parts along dimension 0, may hold values from -6 to 6
- memory_arrays: float32 [256, 32, 64, 64], P(('grp', 'ep'), 'tp'), parts along dimension 0, may hold values from -4 to 4
- chosen_specialist: int32 [256, 2], P(('grp', 'ep')), parts along dimension 0, may hold values from 0 to 3, all different within a row; in each aligned block of 128 rows (0 to 127, 128 to 255, ...) at most 96 rows name the same one
- chosen_coefficient: bfloat16 [256, 2], P(('grp', 'ep')), parts along dimension 0, may hold values from 0.25 to 1
- first_rescale: float32 [2048], replicated, may hold values from 0.1 to 1.9
- second_rescale: float32 [2048], replicated, may hold values from 0.1 to 1.9
- receiver_projector: bfloat16 [2048, 2048], P('tp', 'ep'), may hold values from -0.125 to 0.125
- address_projector: bfloat16 [2048, 2048], P('tp', 'ep'), may hold values from -0.125 to 0.125
- content_projector: bfloat16 [2048, 2048], P('tp', 'ep'), may hold values from -0.125 to 0.125
- final_projector: bfloat16 [2048, 2048], P('tp', 'ep'), may hold values from -0.125 to 0.125
- forget_narrowing: bfloat16 [2048, 64], replicated, may hold values from -0.125 to 0.125
- forget_widening: bfloat16 [64, 2048], P(None, 'tp'), may hold values from -0.75 to 0.75
- forget_bias: float32 [2048], P('tp'), may hold values from -3 to 1
- learning_narrowing: bfloat16 [2048, 64], replicated, may hold values from -0.125 to 0.125
- learning_widening: bfloat16 [64, 2048], P(None, 'tp'), may hold values from -0.75 to 0.75
- learning_bias: float32 [2048], P('tp'), may hold values from -1.5 to 1.5
- lane_scaling: float32 [2048], P('tp'), may hold values from 0.1 to 1.9
- instant_reward: float32 [32, 64], P('tp'), may hold values from -0.5 to 0.5
- specialist_switch: bfloat16 [2048, 28672], P(None, ('ep', 'tp')), may hold values from -0.125 to 0.125
- specialist_expand: bfloat16 [2048, 28672], P(None, ('ep', 'tp')), may hold values from -0.125 to 0.125
- specialist_contract: bfloat16 [28672, 2048], P(('ep', 'tp')), may hold values from -0.0625 to 0.0625
- common_activator: bfloat16 [2048, 5632], P(None, ('ep', 'tp')), may hold values from -0.125 to 0.125
- common_expand: bfloat16 [2048, 5632], P(None, ('ep', 'tp')), may hold values from -0.125 to 0.125
- common_contract: bfloat16 [5632, 2048], P(('ep', 'tp')), may hold values from -0.078125 to 0.078125
- common_switch: bfloat16 [2048], replicated, may hold values from -0.125 to 0.125
Outputs:
- new_tokens: bfloat16 [256, 2048], P(('grp', 'ep', 'tp')), parts along dimension 0
- memory_after: float32 [256, 32, 64, 64], P(('grp', 'ep'), 'tp'), parts along dimension 0
There are 2 independent parts, one for each index of `grp`. A program takes and returns all parts, laid end to end along the dimension named above; an argument that names none is the same for every part. Nothing has to cross between parts.
Inputs may be any that keep to these rules, and one draw needn't show every extreme that they name: `chosen_specialist`: each row names 2 different experts. Over the whole batch no expert is named by more than 96 rows, and in every draw some expert is named by exactly 96 rows.
All inputs are finite; a program needn't handle non-finite values.
Results may differ from a plain program's by a relative error of at most 0.014.
Values may be sent and summed in bfloat16 or wider, within the bound.
A program may use at most 128 MiB of HBM per device.

v0:
```python
import jax
import jax.numpy as jnp
from jax import lax
from jax.sharding import PartitionSpec as P

LANE_WIDTH = 64
FF_E = 7168
RMS_EPS = 1e-06
GROUP_EPS = 0.00064
HIGHEST = lax.Precision.HIGHEST


def rms_norm(values, norm_gain):
    mean_sq = jnp.mean(values * values, axis=-1, keepdims=True)
    return values * lax.rsqrt(mean_sq + RMS_EPS) * norm_gain


def widen(rounded):
    return lax.optimization_barrier(rounded).astype(jnp.float32)


def evolve_memory(
    memory_arrays,
    receiver_lanes,
    address_lanes,
    content_lanes,
    forget_lanes,
    learning_lanes,
    lane_rescale,
    instant_reward,
):
    unit_key = address_lanes * lax.rsqrt(
        jnp.sum(address_lanes * address_lanes, axis=-1, keepdims=True) + 1.0
    )
    stepped_address = address_lanes * learning_lanes
    removal = jnp.einsum("bhvk,bhk->bhv", memory_arrays, unit_key, precision=HIGHEST)
    memory_after = (
        memory_arrays * forget_lanes[:, :, None, :]
        - removal[..., None] * (unit_key * learning_lanes)[:, :, None, :]
        + content_lanes[..., None] * stepped_address[:, :, None, :]
    )
    memory_retrieval = jnp.einsum("bhvk,bhk->bhv", memory_after, receiver_lanes, precision=HIGHEST)
    centred = memory_retrieval - jnp.mean(memory_retrieval, axis=-1, keepdims=True)
    unit_address = centred * lax.rsqrt(
        jnp.mean(centred * centred, axis=-1, keepdims=True) + GROUP_EPS
    )
    instant_extra = (
        jnp.sum(receiver_lanes * stepped_address * instant_reward, axis=-1, keepdims=True)
        * content_lanes
    )
    return (memory_after, unit_address * lane_rescale + instant_extra)


def swiglu(rows_in, gate_w, up_w):
    gate_val = jnp.dot(rows_in, gate_w, preferred_element_type=jnp.float32)
    up_val = jnp.dot(rows_in, up_w, preferred_element_type=jnp.float32)
    return (jax.nn.silu(gate_val) * up_val).astype(jnp.bfloat16)


def body(
    fresh_inputs,
    memory_arrays,
    chosen_specialist,
    chosen_coefficient,
    first_rescale,
    second_rescale,
    receiver_projector,
    address_projector,
    content_projector,
    final_projector,
    forget_narrowing,
    forget_widening,
    forget_bias,
    learning_narrowing,
    learning_widening,
    learning_bias,
    lane_scaling,
    instant_reward,
    specialist_switch,
    specialist_expand,
    specialist_contract,
    common_activator,
    common_expand,
    common_contract,
    common_switch,
):
    own_rows = fresh_inputs.shape[0]
    model_width = fresh_inputs.shape[1]
    tp_count = lax.axis_size("tp")
    tp_rank = lax.axis_index("tp")
    half_width = model_width // tp_count
    head_count = half_width // LANE_WIDTH
    residual = fresh_inputs.astype(jnp.float32)
    normed = rms_norm(residual, first_rescale).astype(jnp.bfloat16)
    normed_half = lax.dynamic_slice_in_dim(normed, tp_rank * half_width, half_width, 1)
    local_weights = jnp.stack((receiver_projector, address_projector, content_projector), axis=1)
    projected_rows = jnp.einsum(
        "rd,dkc->rkc",
        lax.all_gather(normed_half, "ep", axis=0, tiled=True),
        local_weights,
        preferred_element_type=jnp.float32,
    ).astype(jnp.bfloat16)
    partial_value = lax.all_to_all(projected_rows, "ep", split_axis=0, concat_axis=2, tiled=True)
    projected = lax.psum(widen(partial_value).astype(jnp.bfloat16), "tp")
    mine = lax.dynamic_slice_in_dim(projected, tp_rank * half_width, half_width, 2)

    def divide_lanes(channels):
        return channels.astype(jnp.float32).reshape(own_rows, head_count, LANE_WIDTH)

    decay_mid = jnp.tanh(
        jnp.dot(normed, forget_narrowing, preferred_element_type=jnp.float32)
    ).astype(jnp.bfloat16)
    decay_pre = forget_bias + jnp.dot(
        decay_mid, forget_widening, preferred_element_type=jnp.float32
    )
    decay_vals = jnp.exp(-jnp.exp(-jax.nn.softplus(-decay_pre) - 0.5))
    rate_mid = jnp.dot(normed, learning_narrowing, preferred_element_type=jnp.float32).astype(
        jnp.bfloat16
    )
    rate_vals = jax.nn.sigmoid(
        learning_bias + jnp.dot(rate_mid, learning_widening, preferred_element_type=jnp.float32)
    )
    memory_after, memory_retrieval = evolve_memory(
        memory_arrays,
        divide_lanes(mine[:, 0]),
        divide_lanes(mine[:, 1]),
        divide_lanes(mine[:, 2]),
        divide_lanes(decay_vals),
        divide_lanes(rate_vals),
        lane_scaling.reshape(head_count, LANE_WIDTH),
        instant_reward,
    )
    attended = memory_retrieval.reshape(own_rows, half_width).astype(jnp.bfloat16)
    done_rows = jnp.dot(
        lax.all_gather(attended, "ep", axis=0, tiled=True),
        final_projector,
        preferred_element_type=jnp.float32,
    ).astype(jnp.bfloat16)
    out_part = lax.all_to_all(done_rows, "ep", split_axis=0, concat_axis=1, tiled=True)
    mixed_out = lax.psum(widen(out_part).astype(jnp.bfloat16), "tp")
    residual = residual + mixed_out.astype(jnp.float32)
    ffn_in = rms_norm(residual, second_rescale).astype(jnp.bfloat16)
    all_in, all_weight, all_ids = (
        lax.all_gather(ffn_in, "ep", axis=0, tiled=True),
        lax.all_gather(chosen_coefficient, "ep", axis=0, tiled=True),
        lax.all_gather(chosen_specialist, "ep", axis=0, tiled=True),
    )
    column_count = specialist_switch.shape[1]
    flat_rank = lax.axis_index("ep") * tp_count + tp_rank
    expert = flat_rank * column_count // FF_E
    expert_share = jnp.sum(
        jnp.where(all_ids == expert, all_weight.astype(jnp.float32), 0.0), axis=1
    )
    hidden = swiglu(all_in, specialist_switch, specialist_expand)
    shared_hidden = swiglu(all_in, common_activator, common_expand)
    branch_scale = jax.nn.sigmoid(
        jnp.dot(all_in, common_switch, preferred_element_type=jnp.float32)
    )
    rows_mine = own_rows // tp_count
    expert_term = expert_share[:, None] * jnp.dot(
        hidden, specialist_contract, preferred_element_type=jnp.float32
    )
    routed = lax.psum_scatter(
        expert_term
        + branch_scale[:, None]
        * jnp.dot(shared_hidden, common_contract, preferred_element_type=jnp.float32),
        ("ep", "tp"),
        scatter_dimension=0,
        tiled=True,
    )
    own_residual = lax.dynamic_slice_in_dim(residual, tp_rank * rows_mine, rows_mine, 0)
    return ((own_residual + routed).astype(jnp.bfloat16), memory_after)


def solution(mesh):
    placed = (
        P(("grp", "ep"), None),
        P(("grp", "ep"), "tp", None, None),
        P(("grp", "ep"), None),
        P(("grp", "ep"), None),
        P(),
        P(),
        P("tp", "ep"),
        P("tp", "ep"),
        P("tp", "ep"),
        P("tp", "ep"),
        P(),
        P(None, "tp"),
        P("tp"),
        P(),
        P(None, "tp"),
        P("tp"),
        P("tp"),
        P("tp", None),
        P(None, ("ep", "tp")),
        P(None, ("ep", "tp")),
        P(("ep", "tp"), None),
        P(None, ("ep", "tp")),
        P(None, ("ep", "tp")),
        P(("ep", "tp"), None),
        P(),
    )
    return jax.shard_map(
        body,
        mesh=mesh,
        in_specs=placed,
        out_specs=(P(("grp", "ep", "tp"), None), P(("grp", "ep"), "tp", None, None)),
        check_vma=False,
    )
```

profile of v0, /device:TPU:0, one launch (start us, length us, event | category | flops | bytes accessed | tf_op | source)
XLA Modules:
  0.0 324.2 jit_solution(6716720031161532944)
XLA Ops:
  7.2 1.1 fusion.33
  8.3 0.9 fusion.35
  9.3 32.6 %all_gather.15 = bf16[128,1024]{1,0:T(8,128)(2,1)S(1)} all-gather(bf16[16,1024]{1,0:T(8,128)(2,1)S(1)} %constant_dynamic-slice_fusion.1), channel_id=1, replica_groups=mesh['grp'=2,'ep'=8,'tp'=2] {'ep'}, dimensions={0}, use_global_device_ids=true | all-gather | bytes 294912 | tf_op jit(solution)/shard_map/all_gather | solution.py:99
  41.8 1.7 fusion.9
  43.6 0.9 copy.30
  44.5 5.5 %all-to-all-start = ((bf16[128,3,256]{2,1,0:T(4,128)(2,1)}), bf16[128,3,256]{2,1,0:T(4,128)(2,1)S(1)}, u32[]{:S(2)}, u32[]{:S(2)}) async-start(bf16[128,3,256]{2,1,0:T(4,128)(2,1)} %copy.30), calls=%async_computation | async-start | bytes 524288 | tf_op jit(solution)/shard_map/all_to_all | solution.py:103
  50.0 1.4 fusion.19
  51.4 0.1 reshape.102
  51.5 6.7 %all-to-all-done = bf16[128,3,256]{2,1,0:T(4,128)(2,1)S(1)} async-done(((bf16[128,3,256]{2,1,0:T(4,128)(2,1)}), bf16[128,3,256]{2,1,0:T(4,128)(2,1)S(1)}, u32[]{:S(2)}, u32[]{:S(2)}) %all-to-all-start) | async-done | bytes 196640 | tf_op jit(solution)/shard_map/all_to_all | solution.py:103
  58.2 0.1 copy.39
  58.3 0.8 all_to_all.30
  59.2 0.4 fusion.42
  59.6 0.1 mul.207
  59.7 0.1 mul.225
  59.7 15.9 %all-reduce.3.cloned.1.call-done = bf16[16,3,2048]{2,0,1:T(8,128)(2,1)} async-done(((bf16[16,3,2048]{2,0,1:T(8,128)(2,1)}), bf16[16,3,2048]{2,0,1:T(8,128)(2,1)}) %all-reduce.3.cloned.1.call-update) | async-done | bytes 196624 | tf_op jit(solution)/shard_map/psum | solution.py:104
  75.7 0.8 constant_dynamic-slice_fusion
  76.5 0.1 reshape.124
  76.6 0.1 reshape.103
  76.7 0.1 reshape.104
  76.8 0.1 multiply_reduce_fusion.2
  76.9 0.1 reshape.105
  77.0 0.1 fusion.48
  77.1 15.4 %fusion.49 = f32[16,16,1,64]{3,2,1,0:T(1,128)S(1)} fusion(f32[16,16,64,1]{2,3,1,0:T(1,128)S(1)} %bitcast.75, f32[16,16,64,64]{3,2,1,0:T(8,128)} %param.26), kind=kOutput, calls=%fused_computation.80 | convolution fusion | flops 12582912 | bytes 4325376 | tf_op jit(solution)/shard_map/bhvk,bhk->bhv/dot_general | solution.py:36
  92.5 8.6 %multiply_add_fusion = f32[16,16,64,64]{3,2,1,0:T(8,128)S(1)} fusion(f32[16,16,64,64]{3,2,1,0:T(8,128)} %param.26, f32[16,16,64]{2,1,0:T(8,128)S(1)} %get-tuple-element.4, f32[16,16,64]{2,1,0:T(8,128)S(1)} %reshape.105, f32[16,16,64]{2,1,0:T(8,128)S(1)} %get-tuple-element.2, f32[16,16,64]{2,1,0:T(8,128)S(1)} %bitcast.74, f32[16,16,64]{2,1,0:T(8,128)S(1)} %mul.207), kind=kLoop, calls=%fused_computation.1 | loop fusion | flops 5242880 | bytes 8716288 | tf_op jit(solution)/shard_map/add | solution.py:38
  101.1 3.4 %copy-done.1 = f32[16,16,64,64]{3,2,1,0:T(8,128)} copy-done((f32[16,16,64,64]{3,2,1,0:T(8,128)}, f32[16,16,64,64]{3,2,1,0:T(8,128)S(1)}, u32[]{:S(2)}) %copy-start.1) | copy-done | bytes 4194328
  104.6 6.6 %fusion.50 = f32[16,16,1,64]{3,2,1,0:T(1,128)S(1)} fusion(f32[16,16,64,64]{3,2,1,0:T(8,128)S(1)} %multiply_add_fusion, bf16[16,16,64,1]{2,3,1,0:T(2,128)(2,1)S(1)} %reshape.124), kind=kOutput, calls=%fused_computation.81 | convolution fusion | flops 12582912 | bytes 4292608 | tf_op jit(solution)/shard_map/bhvk,bhk->bhv/dot_general | solution.py:42
  111.2 0.1 reduce_sum.65
  111.3 0.2 multiply_reduce_fusion.1
  111.5 0.5 fusion.15
  112.0 0.1 convert_element_type.98
  112.2 31.1 %all_gather.16 = bf16[128,1024]{1,0:T(8,128)(2,1)S(1)} all-gather(bf16[16,1024]{1,0:T(8,128)(2,1)S(1)} %convert_element_type.98), channel_id=1, replica_groups=mesh['grp'=2,'ep'=8,'tp'=2] {'ep'}, dimensions={0}, use_global_device_ids=true | all-gather | bytes 294912 | tf_op jit(solution)/shard_map/all_gather | solution.py:135
  143.3 0.8 convolution_convert_fusion
  144.1 5.4 %all-to-all-start.1 = ((bf16[8,16,256]{2,1,0:T(8,128)(2,1)}), bf16[8,16,256]{2,1,0:T(8,128)(2,1)S(1)}, u32[]{:S(2)}, u32[]{:S(2)}) async-start(bf16[8,16,256]{2,1,0:T(8,128)(2,1)} %bitcast.12), calls=%async_computation.1 | async-start | bytes 131072 | tf_op jit(solution)/shard_map/all_to_all | solution.py:139
  149.6 20.9 %all-gather.1 = bf16[8,16,2]{1,2,0:T(2,128)(2,1)S(1)} all-gather(bf16[1,16,2]{1,2,0:T(2,128)(2,1)S(1)} %bitcast.79), channel_id=1, replica_groups=mesh['grp'=2,'ep'=8,'tp'=2] {'ep'}, dimensions={0}, use_global_device_ids=true | all-gather | bytes 576 | tf_op jit(solution)/shard_map/all_gather | solution.py:145
  170.6 16.5 %all-gather = s32[8,16,2]{1,2,0:T(2,128)S(1)} all-gather(s32[1,16,2]{1,2,0:T(2,128)S(1)} %bitcast.78), channel_id=1, replica_groups=mesh['grp'=2,'ep'=8,'tp'=2] {'ep'}, dimensions={0}, use_global_device_ids=true | all-gather | bytes 1152 | tf_op jit(solution)/shard_map/all_gather | solution.py:146
  187.0 0.6 copy.37
  187.7 0.1 reshape.115
  187.8 16.4 %all-reduce.5.cloned.1.call-done = bf16[16,2048]{1,0:T(8,128)(2,1)} async-done(((bf16[16,2048]{1,0:T(8,128)(2,1)}), bf16[16,2048]{1,0:T(8,128)(2,1)}) %all-reduce.5.cloned.1.call-update) | async-done | bytes 65552 | tf_op jit(solution)/shard_map/psum | solution.py:140
  204.2 1.0 convert_add_fusion
  205.2 0.9 multiply_convert_fusion
  206.1 31.8 %all_gather.19 = bf16[128,2048]{1,0:T(8,128)(2,1)S(1)} all-gather(bf16[16,2048]{1,0:T(8,128)(2,1)S(1)} %multiply_convert_fusion), channel_id=1, replica_groups=mesh['grp'=2,'ep'=8,'tp'=2] {'ep'}, dimensions={0}, use_global_device_ids=true | all-gather | bytes 589824 | tf_op jit(solution)/shard_map/all_gather | solution.py:144
  237.9 5.3 %fusion.51 = f32[128,1792]{1,0:T(8,128)} fusion(bf16[128,2048]{1,0:T(8,128)(2,1)S(1)} %all_gather.19, bf16[2048,1792]{1,0:T(8,128)(2,1)} %param.43), kind=kOutput, calls=%fused_computation.82 | convolution fusion | flops 939524096 | bytes 8781824 | tf_op jit(solution)/shard_map/dot_general | solution.py:55
  243.2 1.2 fusion.52
  244.4 0.2 fusion.25
  244.7 9.1 %convolution_multiply_fusion.1 = f32[128,2048]{1,0:T(8,128)} fusion(bf16[1792,2048]{1,0:T(8,128)(2,1)} %param.45, bf16[128,2048]{1,0:T(8,128)(2,1)S(1)} %all_gather.19, bf16[2048,1792]{1,0:T(8,128)(2,1)} %param.44, f32[128,1792]{1,0:T(8,128)} %fusion.51, f32[128]{0:T(128)S(1)} %reshape.115), kind=kOutput, calls=%fused_computation.3 | convolution fusion | flops 1880686592 | bytes 17170944 | tf_op jit(solution)/shard_map/dot_general | solution.py:160
  253.7 3.8 %fusion.1 = f32[128,2048]{1,0:T(8,128)} fusion(f32[128,2048]{1,0:T(8,128)} %convolution_multiply_fusion.1, bf16[352,2048]{1,0:T(8,128)(2,1)S(1)} %copy-done, bf16[128,2048]{1,0:T(8,128)(2,1)S(1)} %all_gather.19, bf16[2048,352]{0,1:T(8,128)(2,1)S(1)} %copy-done.3, f32[128]{0:T(128)S(1)} %fusion.25, f32[128,352]{0,1:T(8,128)} %fusion.52), kind=kOutput, calls=%fused_computation.5 | convolution fusion | flops 369893376 | bytes 5685760 | tf_op jit(solution)/shard_map/dot_general | solution.py:166
  257.6 58.6 %reduce-scatter.2.cloned.1.call-done = f32[8,2048]{1,0:T(8,128)} async-done(((f32[128,2048]{1,0:T(8,128)}), f32[8,2048]{1,0:T(8,128)}) %reduce-scatter.2.cloned.1.call-update) | async-done | bytes 65552 | tf_op jit(solution)/shard_map/reduce_scatter | solution.py:163
  316.2 1.5 add_convert_fusion
  (44 shorter events, 0.3 us)
Async XLA Ops:
  7.2 246.6 %copy-start = (bf16[352,2048]{1,0:T(8,128)(2,1)S(1)}, bf16[352,2048]{1,0:T(8,128)(2,1)}, u32[]{:S(2)}) copy-start(bf16[352,2048]{1,0:T(8,128)(2,1)} %param.48) | copy-start | bytes 4325380
  7.2 52.0 %copy-start.6 = (bf16[2048,64]{0,1:T(8,128)(2,1)S(1)}, bf16[2048,64]{0,1:T(8,128)(2,1)}, u32[]{:S(2)}) copy-start(bf16[2048,64]{0,1:T(8,128)(2,1)} %param.35) | copy-start | bytes 786436
  7.2 52.0 %copy-start.7 = (bf16[64,1024]{1,0:T(8,128)(2,1)S(1)}, bf16[64,1024]{1,0:T(8,128)(2,1)}, u32[]{:S(2)}) copy-start(bf16[64,1024]{1,0:T(8,128)(2,1)} %param.36) | copy-start | bytes 393220
  7.2 52.0 %copy-start.10 = (f32[1024]{0:T(1024)S(1)}, f32[1024]{0:T(1024)}, u32[]{:S(2)}) copy-start(f32[1024]{0:T(1024)} %param.37) | copy-start | bytes 12292
  7.2 52.5 %copy-start.11 = (f32[1024]{0:T(1024)S(1)}, f32[1024]{0:T(1024)}, u32[]{:S(2)}) copy-start(f32[1024]{0:T(1024)} %param.41) | copy-start | bytes 12292
  44.5 13.7 %all-to-all-start = ((bf16[128,3,256]{2,1,0:T(4,128)(2,1)}), bf16[128,3,256]{2,1,0:T(4,128)(2,1)S(1)}, u32[]{:S(2)}, u32[]{:S(2)}) async-start(bf16[128,3,256]{2,1,0:T(4,128)(2,1)} %copy.30), calls=%async_computation | async-start | bytes 524288 | tf_op jit(solution)/shard_map/all_to_all | solution.py:103
  50.0 25.7 %all-reduce.3.cloned.1.call-start = ((), (), s32[]{:S(2)}) async-start(), calls=%async_computation.3 | async-start | bytes 393216 | tf_op jit(solution)/shard_map/psum | solution.py:104
  101.1 3.4 %copy-start.1 = (f32[16,16,64,64]{3,2,1,0:T(8,128)}, f32[16,16,64,64]{3,2,1,0:T(8,128)S(1)}, u32[]{:S(2)}) copy-start(f32[16,16,64,64]{3,2,1,0:T(8,128)S(1)} %multiply_add_fusion) | copy-start | bytes 12582916
  104.5 7.0 %copy-start.8 = (f32[16,64]{1,0:T(8,128)S(1)}, f32[16,64]{1,0:T(8,128)}, u32[]{:S(2)}) copy-start(f32[16,64]{1,0:T(8,128)} %param.42) | copy-start | bytes 12292
  104.5 38.8 %copy-start.5 = (bf16[1024,256]{1,0:T(8,128)(2,1)S(1)}, bf16[1024,256]{1,0:T(8,128)(2,1)}, u32[]{:S(2)}) copy-start(bf16[1024,256]{1,0:T(8,128)(2,1)} %param.34) | copy-start | bytes 1572868
  104.5 45.1 %copy-start.14 = (bf16[16,2]{0,1:T(2,128)(2,1)S(1)}, bf16[16,2]{0,1:T(2,128)(2,1)}, u32[]{:S(2)}) copy-start(bf16[16,2]{0,1:T(2,128)(2,1)} %param.28) | copy-start | bytes 196
  104.5 66.0 %copy-start.13 = (s32[16,2]{0,1:T(2,128)S(1)}, s32[16,2]{0,1:T(2,128)}, u32[]{:S(2)}) copy-start(s32[16,2]{0,1:T(2,128)} %param.27) | copy-start | bytes 388
  104.5 83.3 %copy-start.12 = (bf16[2048]{0:T(1024)(128)(2,1)S(1)}, bf16[2048]{0:T(1024)(128)(2,1)}, u32[]{:S(2)}) copy-start(bf16[2048]{0:T(1024)(128)(2,1)} %param.49) | copy-start | bytes 12292
  104.5 99.7 %copy-start.4 = (bf16[16,2048]{1,0:T(8,128)(2,1)S(1)}, bf16[16,2048]{1,0:T(8,128)(2,1)}, u32[]{:S(2)}) copy-start(bf16[16,2048]{1,0:T(8,128)(2,1)} %param.25) | copy-start | bytes 196612
  104.5 100.7 %copy-start.9 = (f32[2048]{0:T(1024)S(1)}, f32[2048]{0:T(1024)}, u32[]{:S(2)}) copy-start(f32[2048]{0:T(1024)} %param.30) | copy-start | bytes 24580
  144.1 42.9 %all-to-all-start.1 = ((bf16[8,16,256]{2,1,0:T(8,128)(2,1)}), bf16[8,16,256]{2,1,0:T(8,128)(2,1)S(1)}, u32[]{:S(2)}, u32[]{:S(2)}) async-start(bf16[8,16,256]{2,1,0:T(8,128)(2,1)} %bitcast.12), calls=%async_computation.1 | async-start | bytes 131072 | tf_op jit(solution)/shard_map/all_to_all | solution.py:139
  149.6 54.7 %all-reduce.5.cloned.1.call-start = ((), (), s32[]{:S(2)}) async-start(), calls=%async_computation.4 | async-start | bytes 131072 | tf_op jit(solution)/shard_map/psum | solution.py:140
  187.7 128.5 %reduce-scatter.2.cloned.1.call-start = ((), (), s32[]{:S(2)}) async-start(), calls=%async_computation.5 | async-start | bytes 1114112 | tf_op jit(solution)/shard_map/reduce_scatter | solution.py:163
  237.9 5.3 %copy-start.2 = (bf16[2048,352]{0,1:T(8,128)(2,1)S(1)}, bf16[2048,352]{0,1:T(8,128)(2,1)}, u32[]{:S(2)}) copy-start(bf16[2048,352]{0,1:T(8,128)(2,1)} %param.46) | copy-start | bytes 4325380
  244.7 9.1 %copy-start.3 = (bf16[2048,352]{0,1:T(8,128)(2,1)S(1)}, bf16[2048,352]{0,1:T(8,128)(2,1)}, u32[]{:S(2)}) copy-start(bf16[2048,352]{0,1:T(8,128)(2,1)} %param.47) | copy-start | bytes 4325380
Sparse Core Ops, SparseCore 0:
  59.3 16.3 all-reduce.2
  187.8 16.3 all-reduce.4
  257.7 58.4 reduce-scatter.1
where the time goes:
time: 325 us; the launch traced here: 324 us
  blocking collectives  133 us (41%)
  waiting for transfers between devices  97.7 us (30%)
  matrix products  46 us (14%)
  other arithmetic  15.8 us (5%)
  between operations  14.1 us (4%)
  starting transfers between devices  11.1 us (3%)
  local copies, waits for them, and re-layouts  6.74 us (2%)
    reduce_scatter x1, waiting for transfers between devices, body(): lax.psum_scatter(expert_term + branch_scale[:, None] * jnp.dot(shared_hid...  58.6 us
    all_gather x1, blocking collectives, body(): lax.all_gather(normed_half, 'ep', axis=0, tiled=True)  32.6 us
    all_gather x1, blocking collectives, body(): lax.all_gather(ffn_in, 'ep', axis=0, tiled=True)  31.8 us
    all_gather x1, blocking collectives, body(): lax.all_gather(attended, 'ep', axis=0, tiled=True)  31.1 us
    all_gather x1, blocking collectives, body(): lax.all_gather(chosen_coefficient, 'ep', axis=0, tiled=True)  20.9 us
    all_gather x1, blocking collectives, body(): lax.all_gather(chosen_specialist, 'ep', axis=0, tiled=True)  16.5 us
    psum x1, waiting for transfers between devices, body(): mixed_out = lax.psum(widen(out_part).astype(jnp.bfloat16), 'tp')  16.4 us
    psum x1, waiting for transfers between devices, body(): projected = lax.psum(widen(partial_value).astype(jnp.bfloat16), 'tp')  15.9 us
  transfers between devices with their start and end apart: 5, of which 4 were waited for; matrix products, arithmetic and copies ran while one was open for 1% of the time, Pallas kernels for 0%

commit v1 on v0

--- a/solution.py
+++ b/solution.py
@@ -8,6 +8,20 @@
 RMS_EPS = 1e-06
 GROUP_EPS = 0.00064
 HIGHEST = lax.Precision.HIGHEST
+
+
+def on_each_block(value, axis, dim, make, out_dim):
+    ways, here, lap = (lax.axis_size(axis), lax.axis_index(axis), value.shape[dim])
+    earlier, later = ([], [])
+    going_up = going_down = value
+    for far in range(ways // 2 + 1):
+        earlier.append(make(going_up, (here - far) % ways * lap))
+        if 0 < far < ways - ways // 2:
+            later.append(make(going_down, (here + far) % ways * lap))
+        going_up = lax.ppermute(going_up, axis, [(d, (d + 1) % ways) for d in range(ways)])
+        going_down = lax.ppermute(going_down, axis, [(d, (d - 1) % ways) for d in range(ways)])
+    line = jnp.concatenate([*earlier[::-1], *later], axis=out_dim)
+    return jnp.roll(line, (here - ways // 2) * earlier[0].shape[out_dim], axis=out_dim)
 
 
 def rms_norm(values, norm_gain):
@@ -94,11 +108,14 @@
     normed = rms_norm(residual, first_rescale).astype(jnp.bfloat16)
     normed_half = lax.dynamic_slice_in_dim(normed, tp_rank * half_width, half_width, 1)
     local_weights = jnp.stack((receiver_projector, address_projector, content_projector), axis=1)
-    projected_rows = jnp.einsum(
-        "rd,dkc->rkc",
-        lax.all_gather(normed_half, "ep", axis=0, tiled=True),
-        local_weights,
-        preferred_element_type=jnp.float32,
+    projected_rows = on_each_block(
+        normed_half,
+        "ep",
+        0,
+        lambda part, start: jnp.einsum(
+            "rd,dkc->rkc", part, local_weights, preferred_element_type=jnp.float32
+        ),
+        0,
     ).astype(jnp.bfloat16)
     partial_value = lax.all_to_all(projected_rows, "ep", split_axis=0, concat_axis=2, tiled=True)
     projected = lax.psum(widen(partial_value).astype(jnp.bfloat16), "tp")

time: 325 us -> 318 us (0.978)
  blocking collectives: 133 us -> 100 us
  starting transfers between devices: 11.1 us -> 26.2 us
  waiting for transfers between devices: 97.7 us -> 109 us
  local copies, waits for them, and re-layouts: 6.74 us -> 3.47 us
    all_gather x1 -> x0, blocking collectives: 32.6 us -> none  [body(): lax.all_gather(normed_half, 'ep', axis=0, tiled=True)]
    ppermute x0 -> x7, starting transfers between devices: none -> 17.2 us  [the longest x3 14.2 us: on_each_block(): lax.ppermute(going_down, axis, [(d, (d - 1) % ways) for d in range(ways)])]
    ppermute x0 -> x7, waiting for transfers between devices: none -> 10.6 us  [the longest x4 10.6 us: on_each_block(): lax.ppermute(going_up, axis, [(d, (d + 1) % ways) for d in range(ways)])]
    unnamed x31 -> x52, local copies, waits for them, and re-layouts: 3.47 us -> 0.17 us
  transfers between devices with their start and end apart: 5 -> 12, of which waited for: 4 -> 8; matrix products, arithmetic and copies ran while one was open for 1% -> 2% of each run, Pallas kernels for 0% -> 0%
where the time goes in v1:
time: 318 us; the launch traced here: 317 us
  waiting for transfers between devices  109 us (34%)
  blocking collectives  100 us (31%)
  matrix products  47.4 us (15%)
  starting transfers between devices  26.2 us (8%)
  other arithmetic  15.8 us (5%)
  between operations  14.2 us (4%)
  local copies, waits for them, and re-layouts  3.47 us (1%)
    reduce_scatter x1, waiting for transfers between devices, body(): lax.psum_scatter(expert_term + branch_scale[:, None] * jnp.dot(shared_hid...  58.6 us
    all_gather x1, blocking collectives, body(): lax.all_gather(ffn_in, 'ep', axis=0, tiled=True)  31.8 us
    all_gather x1, blocking collectives, body(): lax.all_gather(attended, 'ep', axis=0, tiled=True)  31.1 us
    all_gather x1, blocking collectives, body(): lax.all_gather(chosen_coefficient, 'ep', axis=0, tiled=True)  20.9 us
    all_gather x1, blocking collectives, body(): lax.all_gather(chosen_specialist, 'ep', axis=0, tiled=True)  16.5 us
    psum x1, waiting for transfers between devices, body(): mixed_out = lax.psum(widen(out_part).astype(jnp.bfloat16), 'tp')  16.4 us
    psum x1, waiting for transfers between devices, body(): projected = lax.psum(widen(partial_value).astype(jnp.bfloat16), 'tp')  16.1 us
    dot_general x1, matrix products, evolve_memory(): jnp.einsum('bhvk,bhk->bhv', memory_arrays, unit_key, precision=HIGHEST)  15.6 us
  transfers between devices with their start and end apart: 12, of which 8 were waited for; matrix products, arithmetic and copies ran while one was open for 2% of the time, Pallas kernels for 0%

profile of v1, /device:TPU:0, one launch (start us, length us, event | category | flops | bytes accessed | tf_op | source)
XLA Modules:
  0.0 316.7 jit_solution(11669022693761636242)
XLA Ops:
  7.2 1.1 fusion.23
  8.3 0.9 fusion.25
  9.3 3.0 collective-permute-start
  12.3 4.9 %collective-permute-done = bf16[16,1024]{1,0:T(8,128)(2,1)S(1)} collective-permute-done((bf16[16,1024]{1,0:T(8,128)(2,1)S(1)}, bf16[16,1024]{1,0:T(8,128)(2,1)S(1)}, u32[]{:S(2)}, u32[]{:S(2)}) %collective-permute-start) | collective-permute-done | bytes 32800 | tf_op jit(solution)/shard_map/ppermute | solution.py:21
  17.2 4.7 %collective-permute-start.4 = (bf16[16,1024]{1,0:T(8,128)(2,1)S(1)}, bf16[16,1024]{1,0:T(8,128)(2,1)S(1)}, u32[]{:S(2)}, u32[]{:S(2)}) collective-permute-start(bf16[16,1024]{1,0:T(8,128)(2,1)S(1)} %constant_dynamic-slice_fusion.1), channel_id=1, source_target_pairs={{0,14},{2,0},{4,2},{6,4},{8,6},{10,8},{12,10},{14,12},{1,15},{3,1}... | collective-permute-start | bytes 98312 | tf_op jit(solution)/shard_map/ppermute | solution.py:22
  22.0 1.9 collective-permute-done.1
  23.9 4.7 %collective-permute-start.5 = (bf16[16,1024]{1,0:T(8,128)(2,1)S(1)}, bf16[16,1024]{1,0:T(8,128)(2,1)S(1)}, u32[]{:S(2)}, u32[]{:S(2)}) collective-permute-start(bf16[16,1024]{1,0:T(8,128)(2,1)S(1)} %collective-permute-done.4), channel_id=1, source_target_pairs={{0,14},{2,0},{4,2},{6,4},{8,6},{10,8},{12,10},{14,12},{1,15},{3,1}... | collective-permute-start | bytes 98312 | tf_op jit(solution)/shard_map/ppermute | solution.py:22
  28.6 1.9 collective-permute-done.2
  30.5 4.7 %collective-permute-start.6 = (bf16[16,1024]{1,0:T(8,128)(2,1)S(1)}, bf16[16,1024]{1,0:T(8,128)(2,1)S(1)}, u32[]{:S(2)}, u32[]{:S(2)}) collective-permute-start(bf16[16,1024]{1,0:T(8,128)(2,1)S(1)} %collective-permute-done.5), channel_id=1, source_target_pairs={{0,14},{2,0},{4,2},{6,4},{8,6},{10,8},{12,10},{14,12},{1,15},{3,1}... | collective-permute-start | bytes 98312 | tf_op jit(solution)/shard_map/ppermute | solution.py:22
  35.2 1.9 collective-permute-done.3
  37.1 1.7 constant_dynamic-update-slice_fusion.15
  38.9 0.3 constant_dynamic-update-slice_fusion.14
  39.2 0.3 constant_dynamic-update-slice_fusion.13
  39.5 0.3 constant_dynamic-update-slice_fusion.12
  39.8 0.3 constant_dynamic-update-slice_fusion.11
  40.2 0.3 constant_dynamic-update-slice_fusion.10
  40.5 0.3 constant_dynamic-update-slice_fusion.9
  40.9 0.3 constant_dynamic-update-slice_fusion.8
  41.3 0.9 copy.30
  42.2 3.4 %all-to-all-start = ((bf16[128,3,256]{2,1,0:T(4,128)(2,1)}), bf16[128,3,256]{2,1,0:T(4,128)(2,1)S(1)}, u32[]{:S(2)}, u32[]{:S(2)}) async-start(bf16[128,3,256]{2,1,0:T(4,128)(2,1)} %copy.30), calls=%async_computation | async-start | bytes 524288 | tf_op jit(solution)/shard_map/all_to_all | solution.py:120
  45.7 0.4 fusion.10
  46.2 7.6 %all-to-all-done = bf16[128,3,256]{2,1,0:T(4,128)(2,1)S(1)} async-done(((bf16[128,3,256]{2,1,0:T(4,128)(2,1)}), bf16[128,3,256]{2,1,0:T(4,128)(2,1)S(1)}, u32[]{:S(2)}, u32[]{:S(2)}) %all-to-all-start) | async-done | bytes 196640 | tf_op jit(solution)/shard_map/all_to_all | solution.py:120
  53.9 0.8 all_to_all.30
  54.8 0.4 fusion.32
  55.3 16.1 %all-reduce.3.cloned.1.call-done = bf16[16,3,2048]{2,0,1:T(8,128)(2,1)} async-done(((bf16[16,3,2048]{2,0,1:T(8,128)(2,1)}), bf16[16,3,2048]{2,0,1:T(8,128)(2,1)}) %all-reduce.3.cloned.1.call-update) | async-done | bytes 196624 | tf_op jit(solution)/shard_map/psum | solution.py:121
  71.4 0.8 constant_dynamic-slice_fusion
  72.9 15.6 %fusion.54 = f32[16,16,1,64]{3,2,1,0:T(1,128)S(1)} fusion(f32[16,16,64,1]{2,3,1,0:T(1,128)S(1)} %bitcast.112, f32[16,16,64,64]{3,2,1,0:T(8,128)} %param.26), kind=kOutput, calls=%fused_computation.105 | convolution fusion | flops 12582912 | bytes 4325376 | tf_op jit(solution)/shard_map/bhvk,bhk->bhv/dot_general | solution.py:50
  88.5 8.6 %multiply_add_fusion = f32[16,16,64,64]{3,2,1,0:T(8,128)S(1)} fusion(f32[16,16,64,64]{3,2,1,0:T(8,128)} %param.26, f32[16,16,64]{2,1,0:T(8,128)S(1)} %get-tuple-element.4, f32[16,16,64]{2,1,0:T(8,128)S(1)} %reshape.105, f32[16,16,64]{2,1,0:T(8,128)S(1)} %get-tuple-element.2, f32[16,16,64]{2,1,0:T(8,128)S(1)} %bitcast.111, f32[16,16,64]{2,1,0:T(8,128)S(1)} %mul.210), kind=kLoop, calls=%fused_computation.1 | loop fusion | flops 5242880 | bytes 8716288 | tf_op jit(solution)/shard_map/add | solution.py:52
  97.1 6.6 %fusion.55 = f32[16,16,1,64]{3,2,1,0:T(1,128)S(1)} fusion(f32[16,16,64,64]{3,2,1,0:T(8,128)S(1)} %multiply_add_fusion, bf16[16,16,64,1]{2,3,1,0:T(2,128)(2,1)S(1)} %reshape.131), kind=kOutput, calls=%fused_computation.106 | convolution fusion | flops 12582912 | bytes 4292608 | tf_op jit(solution)/shard_map/bhvk,bhk->bhv/dot_general | solution.py:56
  103.8 0.2 multiply_reduce_fusion.1
  104.1 0.5 fusion.6
  104.7 31.1 %all_gather.12 = bf16[128,1024]{1,0:T(8,128)(2,1)S(1)} all-gather(bf16[16,1024]{1,0:T(8,128)(2,1)S(1)} %convert_element_type.98), channel_id=1, replica_groups=mesh['grp'=2,'ep'=8,'tp'=2] {'ep'}, dimensions={0}, use_global_device_ids=true | all-gather | bytes 294912 | tf_op jit(solution)/shard_map/all_gather | solution.py:152
  135.8 0.9 convolution_convert_fusion
  136.7 5.4 %all-to-all-start.1 = ((bf16[8,16,256]{2,1,0:T(8,128)(2,1)}), bf16[8,16,256]{2,1,0:T(8,128)(2,1)S(1)}, u32[]{:S(2)}, u32[]{:S(2)}) async-start(bf16[8,16,256]{2,1,0:T(8,128)(2,1)} %bitcast.19), calls=%async_computation.1 | async-start | bytes 131072 | tf_op jit(solution)/shard_map/all_to_all | solution.py:156
  142.2 20.9 %all-gather.1 = bf16[8,16,2]{1,2,0:T(2,128)(2,1)S(1)} all-gather(bf16[1,16,2]{1,2,0:T(2,128)(2,1)S(1)} %bitcast.116), channel_id=1, replica_groups=mesh['grp'=2,'ep'=8,'tp'=2] {'ep'}, dimensions={0}, use_global_device_ids=true | all-gather | bytes 576 | tf_op jit(solution)/shard_map/all_gather | solution.py:162
  163.1 16.5 %all-gather = s32[8,16,2]{1,2,0:T(2,128)S(1)} all-gather(s32[1,16,2]{1,2,0:T(2,128)S(1)} %bitcast.115), channel_id=1, replica_groups=mesh['grp'=2,'ep'=8,'tp'=2] {'ep'}, dimensions={0}, use_global_device_ids=true | all-gather | bytes 1152 | tf_op jit(solution)/shard_map/all_gather | solution.py:163
  179.6 0.6 copy.37
  180.4 16.4 %all-reduce.5.cloned.1.call-done = bf16[16,2048]{1,0:T(8,128)(2,1)} async-done(((bf16[16,2048]{1,0:T(8,128)(2,1)}), bf16[16,2048]{1,0:T(8,128)(2,1)}) %all-reduce.5.cloned.1.call-update) | async-done | bytes 65552 | tf_op jit(solution)/shard_map/psum | solution.py:157
  196.8 1.0 convert_add_fusion
  197.8 0.9 multiply_convert_fusion
  198.8 31.8 %all_gather.15 = bf16[128,2048]{1,0:T(8,128)(2,1)S(1)} all-gather(bf16[16,2048]{1,0:T(8,128)(2,1)S(1)} %multiply_convert_fusion), channel_id=1, replica_groups=mesh['grp'=2,'ep'=8,'tp'=2] {'ep'}, dimensions={0}, use_global_device_ids=true | all-gather | bytes 589824 | tf_op jit(solution)/shard_map/all_gather | solution.py:161
  230.5 5.3 %fusion.56 = f32[128,1792]{1,0:T(8,128)} fusion(bf16[128,2048]{1,0:T(8,128)(2,1)S(1)} %all_gather.15, bf16[2048,1792]{1,0:T(8,128)(2,1)} %param.43), kind=kOutput, calls=%fused_computation.107 | convolution fusion | flops 939524096 | bytes 8781824 | tf_op jit(solution)/shard_map/dot_general | solution.py:69
  235.8 1.2 fusion.57
  237.0 0.2 fusion.16
  237.2 9.1 %convolution_multiply_fusion.1 = f32[128,2048]{1,0:T(8,128)} fusion(bf16[1792,2048]{1,0:T(8,128)(2,1)} %param.45, bf16[128,2048]{1,0:T(8,128)(2,1)S(1)} %all_gather.15, bf16[2048,1792]{1,0:T(8,128)(2,1)} %param.44, f32[128,1792]{1,0:T(8,128)} %fusion.56, f32[128]{0:T(128)S(1)} %reshape.115), kind=kOutput, calls=%fused_computation.3 | convolution fusion | flops 1880686592 | bytes 17170944 | tf_op jit(solution)/shard_map/dot_general | solution.py:177
  246.3 3.8 %fusion.1 = f32[128,2048]{1,0:T(8,128)} fusion(f32[128,2048]{1,0:T(8,128)} %convolution_multiply_fusion.1, bf16[352,2048]{1,0:T(8,128)(2,1)S(1)} %copy-done, bf16[128,2048]{1,0:T(8,128)(2,1)S(1)} %all_gather.15, bf16[2048,352]{0,1:T(8,128)(2,1)S(1)} %copy-done.3, f32[128]{0:T(128)S(1)} %fusion.16, f32[128,352]{0,1:T(8,128)} %fusion.57), kind=kOutput, calls=%fused_computation.5 | convolution fusion | flops 369893376 | bytes 5685760 | tf_op jit(solution)/shard_map/dot_general | solution.py:183
  250.1 58.6 %reduce-scatter.2.cloned.1.call-done = f32[8,2048]{1,0:T(8,128)} async-done(((f32[128,2048]{1,0:T(8,128)}), f32[8,2048]{1,0:T(8,128)}) %reduce-scatter.2.cloned.1.call-update) | async-done | bytes 65552 | tf_op jit(solution)/shard_map/reduce_scatter | solution.py:180
  308.8 1.5 add_convert_fusion
  (87 shorter events, 1.8 us)
Async XLA Ops:
  7.2 239.2 %copy-start = (bf16[352,2048]{1,0:T(8,128)(2,1)S(1)}, bf16[352,2048]{1,0:T(8,128)(2,1)}, u32[]{:S(2)}) copy-start(bf16[352,2048]{1,0:T(8,128)(2,1)} %param.48) | copy-start | bytes 4325380
  7.2 31.7 %copy-start.16 = (bf16[1024,256]{1,0:T(8,128)(2,1)S(1)}, bf16[1024,256]{1,0:T(8,128)(2,1)}, u32[]{:S(2)}) copy-start(bf16[1024,256]{1,0:T(8,128)(2,1)} %param.32) | copy-start | bytes 1572868
  7.2 31.7 %copy-start.15 = (bf16[1024,256]{1,0:T(8,128)(2,1)S(1)}, bf16[1024,256]{1,0:T(8,128)(2,1)}, u32[]{:S(2)}) copy-start(bf16[1024,256]{1,0:T(8,128)(2,1)} %param.33) | copy-start | bytes 1572868
  9.3 8.0 %collective-permute-start = (bf16[16,1024]{1,0:T(8,128)(2,1)S(1)}, bf16[16,1024]{1,0:T(8,128)(2,1)S(1)}, u32[]{:S(2)}, u32[]{:S(2)}) collective-permute-start(bf16[16,1024]{1,0:T(8,128)(2,1)S(1)} %constant_dynamic-slice_fusion.1), channel_id=1, source_target_pairs={{0,2},{2,4},{4,6},{6,8},{8,10},{10,12},{12,14},{14,0},{1,3},{3,5},... | collective-permute-start | bytes 98312 | tf_op jit(solution)/shard_map/ppermute | solution.py:21
  17.2 6.6 %collective-permute-start.1 = (bf16[16,1024]{1,0:T(8,128)(2,1)S(1)}, bf16[16,1024]{1,0:T(8,128)(2,1)S(1)}, u32[]{:S(2)}, u32[]{:S(2)}) collective-permute-start(bf16[16,1024]{1,0:T(8,128)(2,1)S(1)} %collective-permute-done), channel_id=1, source_target_pairs={{0,2},{2,4},{4,6},{6,8},{8,10},{10,12},{12,14},{14,0},{1,3},{3,5},... | collective-permute-start | bytes 98312 | tf_op jit(solution)/shard_map/ppermute | solution.py:21
  17.2 6.6 %collective-permute-start.4 = (bf16[16,1024]{1,0:T(8,128)(2,1)S(1)}, bf16[16,1024]{1,0:T(8,128)(2,1)S(1)}, u32[]{:S(2)}, u32[]{:S(2)}) collective-permute-start(bf16[16,1024]{1,0:T(8,128)(2,1)S(1)} %constant_dynamic-slice_fusion.1), channel_id=1, source_target_pairs={{0,14},{2,0},{4,2},{6,4},{8,6},{10,8},{12,10},{14,12},{1,15},{3,1}... | collective-permute-start | bytes 98312 | tf_op jit(solution)/shard_map/ppermute | solution.py:22
  23.9 6.6 %collective-permute-start.2 = (bf16[16,1024]{1,0:T(8,128)(2,1)S(1)}, bf16[16,1024]{1,0:T(8,128)(2,1)S(1)}, u32[]{:S(2)}, u32[]{:S(2)}) collective-permute-start(bf16[16,1024]{1,0:T(8,128)(2,1)S(1)} %collective-permute-done.1), channel_id=1, source_target_pairs={{0,2},{2,4},{4,6},{6,8},{8,10},{10,12},{12,14},{14,0},{1,3},{3,5},... | collective-permute-start | bytes 98312 | tf_op jit(solution)/shard_map/ppermute | solution.py:21
  23.9 6.6 %collective-permute-start.5 = (bf16[16,1024]{1,0:T(8,128)(2,1)S(1)}, bf16[16,1024]{1,0:T(8,128)(2,1)S(1)}, u32[]{:S(2)}, u32[]{:S(2)}) collective-permute-start(bf16[16,1024]{1,0:T(8,128)(2,1)S(1)} %collective-permute-done.4), channel_id=1, source_target_pairs={{0,14},{2,0},{4,2},{6,4},{8,6},{10,8},{12,10},{14,12},{1,15},{3,1}... | collective-permute-start | bytes 98312 | tf_op jit(solution)/shard_map/ppermute | solution.py:22
  30.5 6.6 %collective-permute-start.3 = (bf16[16,1024]{1,0:T(8,128)(2,1)S(1)}, bf16[16,1024]{1,0:T(8,128)(2,1)S(1)}, u32[]{:S(2)}, u32[]{:S(2)}) collective-permute-start(bf16[16,1024]{1,0:T(8,128)(2,1)S(1)} %collective-permute-done.2), channel_id=1, source_target_pairs={{0,2},{2,4},{4,6},{6,8},{8,10},{10,12},{12,14},{14,0},{1,3},{3,5},... | collective-permute-start | bytes 98312 | tf_op jit(solution)/shard_map/ppermute | solution.py:21
  30.5 8.4 %copy-start.18 = (bf16[1024,256]{1,0:T(8,128)(2,1)S(1)}, bf16[1024,256]{1,0:T(8,128)(2,1)}, u32[]{:S(2)}) copy-start(bf16[1024,256]{1,0:T(8,128)(2,1)} %param.31) | copy-start | bytes 1572868
  30.5 10.3 %collective-permute-start.6 = (bf16[16,1024]{1,0:T(8,128)(2,1)S(1)}, bf16[16,1024]{1,0:T(8,128)(2,1)S(1)}, u32[]{:S(2)}, u32[]{:S(2)}) collective-permute-start(bf16[16,1024]{1,0:T(8,128)(2,1)S(1)} %collective-permute-done.5), channel_id=1, source_target_pairs={{0,14},{2,0},{4,2},{6,4},{8,6},{10,8},{12,10},{14,12},{1,15},{3,1}... | collective-permute-start | bytes 98312 | tf_op jit(solution)/shard_map/ppermute | solution.py:22
  37.1 2.1 copy-start.17
  40.8 4.9 %copy-start.19 = (bf16[2048,64]{0,1:T(8,128)(2,1)S(1)}, bf16[2048,64]{0,1:T(8,128)(2,1)}, u32[]{:S(2)}) copy-start(bf16[2048,64]{0,1:T(8,128)(2,1)} %param.38) | copy-start | bytes 786436
  40.8 4.9 %copy-start.20 = (bf16[64,1024]{1,0:T(8,128)(2,1)S(1)}, bf16[64,1024]{1,0:T(8,128)(2,1)}, u32[]{:S(2)}) copy-start(bf16[64,1024]{1,0:T(8,128)(2,1)} %param.39) | copy-start | bytes 393220
  40.8 4.9 %copy-start.21 = (f32[1024]{0:T(1024)S(1)}, f32[1024]{0:T(1024)}, u32[]{:S(2)}) copy-start(f32[1024]{0:T(1024)} %param.40) | copy-start | bytes 12292
  40.8 13.9 %copy-start.6 = (bf16[2048,64]{0,1:T(8,128)(2,1)S(1)}, bf16[2048,64]{0,1:T(8,128)(2,1)}, u32[]{:S(2)}) copy-start(bf16[2048,64]{0,1:T(8,128)(2,1)} %param.35) | copy-start | bytes 786436
  40.9 13.9 %copy-start.7 = (bf16[64,1024]{1,0:T(8,128)(2,1)S(1)}, bf16[64,1024]{1,0:T(8,128)(2,1)}, u32[]{:S(2)}) copy-start(bf16[64,1024]{1,0:T(8,128)(2,1)} %param.36) | copy-start | bytes 393220
  40.9 13.9 %copy-start.10 = (f32[1024]{0:T(1024)S(1)}, f32[1024]{0:T(1024)}, u32[]{:S(2)}) copy-start(f32[1024]{0:T(1024)} %param.37) | copy-start | bytes 12292
  40.9 14.4 %copy-start.11 = (f32[1024]{0:T(1024)S(1)}, f32[1024]{0:T(1024)}, u32[]{:S(2)}) copy-start(f32[1024]{0:T(1024)} %param.41) | copy-start | bytes 12292
  42.2 11.6 %all-to-all-start = ((bf16[128,3,256]{2,1,0:T(4,128)(2,1)}), bf16[128,3,256]{2,1,0:T(4,128)(2,1)S(1)}, u32[]{:S(2)}, u32[]{:S(2)}) async-start(bf16[128,3,256]{2,1,0:T(4,128)(2,1)} %copy.30), calls=%async_computation | async-start | bytes 524288 | tf_op jit(solution)/shard_map/all_to_all | solution.py:120
  45.6 25.8 %all-reduce.3.cloned.1.call-start = ((), (), s32[]{:S(2)}) async-start(), calls=%async_computation.3 | async-start | bytes 393216 | tf_op jit(solution)/shard_map/psum | solution.py:121
  97.0 6.7 %copy-start.1 = (f32[16,16,64,64]{3,2,1,0:T(8,128)}, f32[16,16,64,64]{3,2,1,0:T(8,128)S(1)}, u32[]{:S(2)}) copy-start(f32[16,16,64,64]{3,2,1,0:T(8,128)S(1)} %multiply_add_fusion) | copy-start | bytes 12582916
  97.0 7.0 %copy-start.8 = (f32[16,64]{1,0:T(8,128)S(1)}, f32[16,64]{1,0:T(8,128)}, u32[]{:S(2)}) copy-start(f32[16,64]{1,0:T(8,128)} %param.42) | copy-start | bytes 12292
  97.0 38.8 %copy-start.5 = (bf16[1024,256]{1,0:T(8,128)(2,1)S(1)}, bf16[1024,256]{1,0:T(8,128)(2,1)}, u32[]{:S(2)}) copy-start(bf16[1024,256]{1,0:T(8,128)(2,1)} %param.34) | copy-start | bytes 1572868
  97.0 45.2 %copy-start.14 = (bf16[16,2]{0,1:T(2,128)(2,1)S(1)}, bf16[16,2]{0,1:T(2,128)(2,1)}, u32[]{:S(2)}) copy-start(bf16[16,2]{0,1:T(2,128)(2,1)} %param.28) | copy-start | bytes 196
  97.1 66.1 %copy-start.13 = (s32[16,2]{0,1:T(2,128)S(1)}, s32[16,2]{0,1:T(2,128)}, u32[]{:S(2)}) copy-start(s32[16,2]{0,1:T(2,128)} %param.27) | copy-start | bytes 388
  97.1 83.4 %copy-start.12 = (bf16[2048]{0:T(1024)(128)(2,1)S(1)}, bf16[2048]{0:T(1024)(128)(2,1)}, u32[]{:S(2)}) copy-start(bf16[2048]{0:T(1024)(128)(2,1)} %param.49) | copy-start | bytes 12292
  97.1 99.7 %copy-start.4 = (bf16[16,2048]{1,0:T(8,128)(2,1)S(1)}, bf16[16,2048]{1,0:T(8,128)(2,1)}, u32[]{:S(2)}) copy-start(bf16[16,2048]{1,0:T(8,128)(2,1)} %param.25) | copy-start | bytes 196612
  97.1 100.7 %copy-start.9 = (f32[2048]{0:T(1024)S(1)}, f32[2048]{0:T(1024)}, u32[]{:S(2)}) copy-start(f32[2048]{0:T(1024)} %param.30) | copy-start | bytes 24580
  136.7 42.9 %all-to-all-start.1 = ((bf16[8,16,256]{2,1,0:T(8,128)(2,1)}), bf16[8,16,256]{2,1,0:T(8,128)(2,1)S(1)}, u32[]{:S(2)}, u32[]{:S(2)}) async-start(bf16[8,16,256]{2,1,0:T(8,128)(2,1)} %bitcast.19), calls=%async_computation.1 | async-start | bytes 131072 | tf_op jit(solution)/shard_map/all_to_all | solution.py:156
  142.1 54.7 %all-reduce.5.cloned.1.call-start = ((), (), s32[]{:S(2)}) async-start(), calls=%async_computation.4 | async-start | bytes 131072 | tf_op jit(solution)/shard_map/psum | solution.py:157
  180.3 128.5 %reduce-scatter.2.cloned.1.call-start = ((), (), s32[]{:S(2)}) async-start(), calls=%async_computation.5 | async-start | bytes 1114112 | tf_op jit(solution)/shard_map/reduce_scatter | solution.py:180
  230.5 5.3 %copy-start.2 = (bf16[2048,352]{0,1:T(8,128)(2,1)S(1)}, bf16[2048,352]{0,1:T(8,128)(2,1)}, u32[]{:S(2)}) copy-start(bf16[2048,352]{0,1:T(8,128)(2,1)} %param.46) | copy-start | bytes 4325380
  237.2 9.1 %copy-start.3 = (bf16[2048,352]{0,1:T(8,128)(2,1)S(1)}, bf16[2048,352]{0,1:T(8,128)(2,1)}, u32[]{:S(2)}) copy-start(bf16[2048,352]{0,1:T(8,128)(2,1)} %param.47) | copy-start | bytes 4325380
Sparse Core Ops, SparseCore 0:
  54.9 16.5 all-reduce.2
  180.4 16.3 all-reduce.4
  250.3 58.4 reduce-scatter.1
